TPU v7x, 32 devices: a whole 2x2x4 slice. The times are simulated.
32 devices in a mesh: ep: 8 (over z, x), tp: 4 (over y, core).
Axes of the slice: x: 2, y: 2, z: 4, core: 2. Of those that a mesh axis runs over, the one named last changes fastest.
Arguments:
- tokens: bfloat16 [256, 2048], P('ep'), may hold values from -6 to 6
- norm_gain: float32 [2048], replicated, may hold values from 0.1 to 1.9
- norm_bias: float32 [2048], replicated, may hold values from -3 to 3
- routes: int32 [256, 4], P('ep'), may hold values from 0 to 7, all different within a row; in each aligned block of 32 rows (0 to 31, 32 to 63, ...) at most 32 rows name the same one
- route_weights: float32 [256, 4], P('ep'), may hold values from 0.2 to 1
- gate_w: bfloat16 [8, 2048, 4096], P('ep', None, 'tp'), may hold values from -0.125 to 0.125
- up_w: bfloat16 [8, 2048, 4096], P('ep', None, 'tp'), may hold values from -0.125 to 0.125
- down_w: bfloat16 [8, 4096, 2048], P('ep', 'tp'), may hold values from -0.09375 to 0.09375
Outputs:
- mixed: bfloat16 [256, 2048], P('ep', 'tp')
Inputs may be any that keep to these rules, and one draw needn't show every extreme that they name: `routes`: the 4 experts of a token differ; the rows of one index of ep name no expert more than 32 times, and in every draw some index of ep names some expert exactly 32 times.
All inputs are finite; a program needn't handle non-finite values.
Results may differ from a plain program's by a relative error of at most 0.017.
Values may be sent and summed in bfloat16 or wider, within the bound.
A program may use at most 64 MiB of HBM per device.

v0:
```python
import functools

import jax
import jax.numpy as jnp
from jax import lax
from jax.experimental import pallas as pl
from jax.experimental.pallas import tpu as pltpu
from jax.sharding import PartitionSpec as P

MESH = pl.DeviceIdType.MESH
LANES = 128


def offsets(count):
    return sorted(range(1, count), key=lambda o: (abs(2 * o - count), o))


def kernel(
    dims, tokens_hbm, gain_hbm, bias_hbm, routes_hbm, weights_hbm, gate_hbm, up_hbm, down_hbm, out_ref,
    tokens, gain, bias, routes, weights,
    buf, gate_v, up_v, down_v, hidden, partial, summed, kept_y, kept_x, from_core, from_y, from_x, from_z,
    input_sem, weight_sem, ag_send, ag_recv, core_send, core_recv, y_send, y_recv, x_send, x_recv, z_send, z_recv,
):
    nz, nx, ny, nc = dims
    f32, bf16 = jnp.float32, jnp.bfloat16
    ep, tp = lax.axis_index("ep"), lax.axis_index("tp")
    z, x = ep // nx, lax.rem(ep, nx)
    y, c = tp // nc, lax.rem(tp, nc)
    other = lax.rem(c + 1, nc)
    groups = 2 if nz % 2 == 0 else 1
    span = nz // groups
    near = (z // span) * span
    lower = z < span

    def along(value, step, count):
        return lax.rem(value + step, count)

    def at(z_index, x_index):
        return (z_index * nx + x_index, tp)

    def x_at(step):
        return along(x, step, nx)

    def at_y(step):
        return (ep, along(y, step, ny) * nc + c)

    partner = (ep, y * nc + other)

    def base(group):
        return near if group == 0 else span - near

    def z_of(group, k):
        if group == 0:
            return near + along(z - near, k, span)
        return jnp.where(lower, span + k, span - 1 - k)

    def chunks(group):
        return list(range(1, span)) + [0] if group == 0 else list(reversed(range(span)))

    others = [z_of(0, k) for k in range(1, span)]
    far = [z_of(1, k) for k in range(span)] if groups == 2 else []

    barrier = pltpu.get_barrier_semaphore()
    greeted = [partner]
    greeted += [at(i, x) for i in far + others]
    greeted += [at(z, x_at(s)) for s in offsets(nx)]
    greeted += [at_y(s) for s in offsets(ny)]
    for target in greeted:
        pl.semaphore_signal(barrier, inc=1, device_id=target, device_id_type=MESH)

    inputs = []
    for i, (hbm, vmem) in enumerate(
        (
            (tokens_hbm, tokens),
            (gain_hbm, gain),
            (bias_hbm, bias),
            (routes_hbm, routes),
            (weights_hbm, weights),
        )
    ):
        load = pltpu.make_async_copy(hbm, vmem, input_sem.at[i])
        load.start()
        inputs.append(load)

    for load in inputs:
        load.wait()
    tiles, tile = gate_v.shape[0], gate_v.shape[2]
    out_tiles, out_tile = down_v.shape[0], down_v.shape[2]
    loads = []
    for i in range(tiles):
        for which, (hbm, vmem) in enumerate(((gate_hbm, gate_v), (up_hbm, up_v))):
            load = pltpu.make_async_copy(
                hbm.at[0, :, pl.ds(i * tile, tile)], vmem.at[i], weight_sem.at[which, i]
            )
            load.start()
            loads.append(load)
    for i in range(out_tiles):
        load = pltpu.make_async_copy(
            down_hbm.at[0, :, pl.ds(i * out_tile, out_tile)], down_v.at[i], weight_sem.at[2, i]
        )
        load.start()
        loads.append(load)

    width = tokens.shape[1]
    half = width // nc
    values = tokens[...].astype(f32)
    centred = values - jnp.mean(values, axis=-1, keepdims=True)
    variance = jnp.mean(centred * centred, axis=-1, keepdims=True)
    normed = (centred * lax.rsqrt(variance + 1e-05) * gain[...] + bias[...]).astype(bf16)
    rows = tokens.shape[0]
    expert = lax.broadcasted_iota(jnp.int32, (LANES, rows), 0)
    mix = jnp.zeros((LANES, rows), f32)
    for k in range(routes.shape[0]):
        mix = mix + jnp.where(routes[k : k + 1, :] == expert, weights[k : k + 1, :], 0.0)
    mix = mix.T
    high = mix.astype(bf16)
    low = (mix - high.astype(f32)).astype(bf16)
    for i in range(nc):
        buf[ep, i, :, 0:half] = normed[:, i * half : (i + 1) * half]
        buf[ep, i, :, half : half + LANES] = high if i == 0 else low
    pl.semaphore_wait(barrier, len(greeted))

    sent = []

    cuts = ag_recv.shape[2]
    cut_rows = rows // cuts

    def piece(source, part, cut):
        if cut is None:
            return buf.at[source, part], ag_recv.at[source, part, 0]
        at_rows = pl.ds(pl.multiple_of(cut * cut_rows, cut_rows), cut_rows)
        return buf.at[source, part, at_rows], ag_recv.at[source, part, cut]

    def forward(source, target, cut=None):
        block, sem = piece(source, c, cut)
        copy = pltpu.make_async_remote_copy(
            src_ref=block,
            dst_ref=block,
            send_sem=ag_send.at[len(sent)],
            recv_sem=sem,
            device_id=target,
            device_id_type=MESH,
        )
        copy.start()
        sent.append(copy)

    def arrived(source, part, cut=None):
        block, sem = piece(source, part, cut)
        pltpu.make_async_remote_copy(
            src_ref=block,
            dst_ref=block,
            send_sem=ag_send.at[0],
            recv_sem=sem,
            device_id=partner,
            device_id_type=MESH,
        ).wait_recv()

    mine = y if cuts > 1 else None

    def share_out(source, cut):
        if cut is not None:
            for s in offsets(ny):
                forward(source, at_y(s), cut)
        forward(source, partner, cut)

    def pass_on(i, cut=None):
        source = i * nx + x
        arrived(source, c, cut)
        for s in offsets(nx):
            forward(source, at(z, x_at(s)), cut)
        share_out(source, cut)

    def hand_over(i, cut=None):
        for s in offsets(nx):
            source = i * nx + x_at(s)
            arrived(source, c, cut)
            share_out(source, cut)

    def collect(i):
        if cuts > 1:
            for t in range(nx):
                source = i * nx + x_at(t)
                for s in offsets(ny):
                    arrived(source, c, along(y, s, ny))
                    forward(source, partner, along(y, s, ny))

    def partner_blocks(i, pieces=1):
        for s in range(nx):
            for cut in range(pieces):
                arrived(i * nx + x_at(s), other, cut if pieces > 1 else None)

    size = span * nx * rows

    def up_phase(group):
        blocks = pl.ds(base(group) * nx, span * nx)
        lanes = lax.broadcasted_iota(jnp.int32, (size, LANES), 1)
        shares = buf[blocks, 0, :, half : half + LANES].astype(f32)
        shares = (shares + buf[blocks, 1, :, half : half + LANES].astype(f32)).reshape(size, LANES)
        share = jnp.sum(jnp.where(lanes == ep, shares, 0.0), axis=1, keepdims=True)

        def step(i, carry):
            gate = jnp.zeros((size, tile), f32)
            up = jnp.zeros((size, tile), f32)
            for part in range(nc):
                block = buf[blocks, part, :, 0:half].reshape(size, half)
                depth = slice(part * half, (part + 1) * half)
                gate = gate + jnp.dot(block, gate_v[i, depth, :], preferred_element_type=f32)
                up = up + jnp.dot(block, up_v[i, depth, :], preferred_element_type=f32)
            hidden[i] = (gate / (1.0 + jnp.exp(-gate)) * up * share).astype(bf16)
            return carry

        lax.fori_loop(0, tiles, step, 0)

    def down_step(group, which):
        acc = jnp.zeros((size, out_tile), f32)
        for i in range(tiles):
            acc = acc + jnp.dot(
                hidden[i], down_v[which, i * tile : (i + 1) * tile, :], preferred_element_type=f32
            )
        partial[group, which] = acc.astype(bf16)

    core_copies, y_copies, x_copies, z_copies = {}, {}, {}, {}

    def down_phase(group):
        for s in offsets(ny) + [0]:
            column = along(y, s, ny)
            down_step(group, column * nc + other)
            copy = pltpu.make_async_remote_copy(
                src_ref=partial.at[group, column * nc + other],
                dst_ref=from_core.at[group, column],
                send_sem=core_send.at[group, column],
                recv_sem=core_recv.at[group, column],
                device_id=partner,
                device_id_type=MESH,
            )
            copy.start()
            core_copies[group, s] = copy
        for s in offsets(ny):
            down_step(group, along(y, s, ny) * nc + c)
        y_phase(group)
        down_step(group, y * nc + c)
        core_copies[group, 0].wait_recv()

    def block_rows(group, k, o):
        place = (z_of(group, k) - base(group)) * nx + x_at(o)
        return pl.ds(pl.multiple_of(place * rows, rows), rows)

    def y_phase(group):
        for s in offsets(ny):
            column = along(y, s, ny)
            core_copies[group, s].wait_recv()
            for o in offsets(nx) + [0]:
                for k in chunks(group):
                    at_rows = block_rows(group, k, o)
                    summed[s - 1, group, k, o] = (
                        partial[group, column * nc + c, at_rows, :].astype(f32)
                        + from_core[group, column, at_rows, :].astype(f32)
                    ).astype(bf16)
                    copy = pltpu.make_async_remote_copy(
                        src_ref=summed.at[s - 1, group, k, o],
                        dst_ref=from_y.at[s - 1, group, k, o],
                        send_sem=y_send.at[s - 1, group, k, o],
                        recv_sem=y_recv.at[s - 1, group, k, o],
                        device_id=at_y(s),
                        device_id_type=MESH,
                    )
                    copy.start()
                    y_copies[s, group, k, o] = copy

    def y_total(group, k, o):
        at_rows = block_rows(group, k, o)
        acc = partial[group, y * nc + c, at_rows, :].astype(f32) + from_core[group, y, at_rows, :].astype(f32)
        for s in offsets(ny):
            y_copies[s, group, k, o].wait_recv()
            acc = acc + from_y[s - 1, group, k, o].astype(f32)
        return acc

    def x_step(group, k):
        for s in offsets(nx):
            kept_y[group, k, s - 1] = y_total(group, k, s).astype(bf16)
            copy = pltpu.make_async_remote_copy(
                src_ref=kept_y.at[group, k, s - 1],
                dst_ref=from_x.at[s - 1, group, k],
                send_sem=x_send.at[s - 1, group, k],
                recv_sem=x_recv.at[s - 1, group, k],
                device_id=at(z, x_at(s)),
                device_id_type=MESH,
            )
            copy.start()
            x_copies[s, group, k] = copy

    def z_step(group, k):
        acc = y_total(group, k, 0)
        for s in offsets(nx):
            x_copies[s, group, k].wait_recv()
            acc = acc + from_x[s - 1, group, k].astype(f32)
        if group == 0 and k == 0:
            return acc
        kept_x[group, k] = acc.astype(bf16)
        copy = pltpu.make_async_remote_copy(
            src_ref=kept_x.at[group, k],
            dst_ref=from_z.at[z],
            send_sem=z_send.at[group, k],
            recv_sem=z_recv.at[z],
            device_id=at(z_of(group, k), x),
            device_id_type=MESH,
        )
        copy.start()
        z_copies[group, k] = copy

    for s in offsets(nx):
        forward(ep, at(z, x_at(s)))
    for i in others:
        forward(ep, at(i, x))
    for i in far:
        forward(ep, at(i, x), mine)
    for s in offsets(nx):
        source = z * nx + x_at(s)
        arrived(source, c)
        forward(source, partner)
    for i in others:
        pass_on(i)
    for i in far:
        pass_on(i, mine)
    for i in others:
        hand_over(i)
    for s in offsets(nx):
        arrived(z * nx + x_at(s), other)
    for i in others:
        partner_blocks(i)
    for load in loads[: 2 * tiles]:
        load.wait()
    up_phase(0)
    for i in far:
        hand_over(i, mine)
    for load in loads[2 * tiles :]:
        load.wait()
    down_phase(0)
    for i in far:
        collect(i)
    if groups == 2:
        for i in far:
            partner_blocks(i, cuts)
        up_phase(1)
    for k in chunks(0):
        x_step(0, k)
    if groups == 2:
        down_phase(1)
        for k in chunks(1):
            x_step(1, k)
    result = None
    for k in chunks(0):
        result = z_step(0, k)
    if groups == 2:
        for k in chunks(1):
            z_step(1, k)
    for i in others + far:
        pltpu.make_async_remote_copy(
            src_ref=from_z.at[i],
            dst_ref=from_z.at[i],
            send_sem=z_send.at[0, 0],
            recv_sem=z_recv.at[i],
            device_id=partner,
            device_id_type=MESH,
        ).wait_recv()
        result = result + from_z[i].astype(f32)
    out_ref[...] = result.astype(out_ref.dtype)

    for copies in (sent, core_copies.values(), y_copies.values(), x_copies.values(), z_copies.values()):
        for copy in copies:
            copy.wait_send()


def body(dims, tokens, norm_gain, norm_bias, routes, route_weights, gate_w, up_w, down_w):
    nz, nx, ny, nc = dims
    rows, width = tokens.shape
    topk = routes.shape[1]
    depth = gate_w.shape[2]
    experts, parts = nz * nx, ny * nc
    groups = 2 if nz % 2 == 0 else 1
    span = nz // groups
    size = span * nx * rows
    tile = min(256, depth)
    out_width = width // parts
    half = width // nc
    bf16, f32 = jnp.bfloat16, jnp.float32
    dma = pltpu.SemaphoreType.DMA
    hbm = pl.BlockSpec(memory_space=pl.ANY)
    y_steps, x_steps = max(ny - 1, 1), max(nx - 1, 1)
    cuts = ny if rows % (16 * ny) == 0 else 1
    ag_sends = nz + nx + (1 + 2 * cuts) * experts
    return pl.pallas_call(
        functools.partial(kernel, dims),
        out_shape=jax.ShapeDtypeStruct((rows, out_width), bf16),
        in_specs=[hbm] * 8,
        out_specs=pl.BlockSpec(memory_space=pltpu.VMEM),
        scratch_shapes=[
            pltpu.VMEM((rows, width), bf16),
            pltpu.VMEM((1, width), f32),
            pltpu.VMEM((1, width), f32),
            pltpu.VMEM((topk, rows), jnp.int32),
            pltpu.VMEM((topk, rows), f32),
            pltpu.VMEM((experts, nc, rows, half + LANES), bf16),
            pltpu.VMEM((depth // tile, width, tile), bf16),
            pltpu.VMEM((depth // tile, width, tile), bf16),
            pltpu.VMEM((parts, depth, out_width), bf16),
            pltpu.VMEM((depth // tile, size, tile), bf16),
            pltpu.VMEM((groups, parts, size, out_width), bf16),
            pltpu.VMEM((y_steps, groups, span, nx, rows, out_width), bf16),
            pltpu.VMEM((groups, span, x_steps, rows, out_width), bf16),
            pltpu.VMEM((groups, span, rows, out_width), bf16),
            pltpu.VMEM((groups, ny, size, out_width), bf16),
            pltpu.VMEM((y_steps, groups, span, nx, rows, out_width), bf16),
            pltpu.VMEM((x_steps, groups, span, rows, out_width), bf16),
            pltpu.VMEM((nz, rows, out_width), bf16),
            dma((5,)),
            dma((3, max(depth // tile, parts))),
            dma((ag_sends,)),
            dma((experts, nc, cuts)),
            dma((groups, ny)),
            dma((groups, ny)),
            dma((y_steps, groups, span, nx)),
            dma((y_steps, groups, span, nx)),
            dma((x_steps, groups, span)),
            dma((x_steps, groups, span)),
            dma((groups, span)),
            dma((nz,)),
        ],
        compiler_params=pltpu.CompilerParams(
            collective_id=0, has_side_effects=True, vmem_limit_bytes=56 * 1024 * 1024
        ),
    )(
        tokens, norm_gain.reshape(1, width), norm_bias.reshape(1, width), routes.T, route_weights.T,
        gate_w, up_w, down_w,
    )


def layout(mesh):
    experts, parts = mesh.shape["ep"], mesh.shape["tp"]
    try:
        places = mesh.devices.reshape(experts, parts)
        across = len({d.coords[0] for d in places[:, 0]})
    except AttributeError:
        across = 2
    across = across if experts % across == 0 else 1
    return experts // across, across, parts // 2, 2


def solution(mesh):
    placed = (
        P("ep", None),
        P(),
        P(),
        P("ep", None),
        P("ep", None),
        P("ep", None, "tp"),
        P("ep", None, "tp"),
        P("ep", "tp", None),
    )
    return jax.shard_map(
        functools.partial(body, layout(mesh)), mesh=mesh, in_specs=placed, out_specs=P("ep", "tp"),
        check_vma=False,
    )
```

profile of v0, /device:TPU:0, one launch (start us, length us, event | category | flops | bytes accessed | tf_op | source)
XLA Modules:
  0.0 35.5 jit_solution(11953125355406252750)
XLA Ops:
  0.0 34.1 %shard_map.82 = bf16[32,512]{1,0:T(8,128)(2,1)} custom-call(bf16[32,2048]{1,0:T(8,128)(2,1)} %tokens_hbm.1, f32[1,2048]{1,0:T(1,128)} %bitcast.4, f32[1,2048]{1,0:T(1,128)} %bitcast.5, s32[4,32]{1,0:T(4,128)} %bitcast.6, f32[4,32]{1,0:T(4,128)} %bitcast.7, bf16[1,2048,1024]{2,1,0:T(8,128)(2,1)} %gate_hbm.1, bf16[1,2048,1024]{2,1,0:T(8,128)(2,1)} %up_hbm.1, ...), custom_call_target="tpu_custom_call" | custom-call | tf_op jit(solution)/shard_map/pallas_call | solution.py:392
  34.1 1.4 %copy.10 = bf16[32,512]{1,0:T(8,128)(2,1)} copy(bf16[32,512]{1,0:T(8,128)(2,1)} %shard_map.82) | data formatting | bytes 65536
where the time goes:
time: 35.7 us; the launch traced here: 35.5 us
  Pallas kernels  34.1 us (96%)
  local copies, waits for them, and re-layouts  1.38 us (4%)
    pallas_call x1, Pallas kernels, body(): pl.pallas_call(functools.partial(kernel, dims), out_shape=jax.ShapeDtypeS...  34.1 us
    unnamed x1, local copies, waits for them, and re-layouts  1.38 us

commit v1 on v0

--- a/solution.py
+++ b/solution.py
@@ -391,7 +391,7 @@
     ag_sends = nz + nx + (1 + 2 * cuts) * experts
     return pl.pallas_call(
         functools.partial(kernel, dims),
-        out_shape=jax.ShapeDtypeStruct((rows, out_width), bf16),
+        out_shape=pltpu.VMEM((rows, out_width), bf16),
         in_specs=[hbm] * 8,
         out_specs=pl.BlockSpec(memory_space=pltpu.VMEM),
         scratch_shapes=[

time: 35.7 us -> 34.3 us (0.961)
  local copies, waits for them, and re-layouts: 1.38 us -> 0.62 us
  Pallas kernels: 34.1 us -> 33.5 us
    unnamed x1, local copies, waits for them, and re-layouts: 1.38 us -> 0.62 us
    pallas_call x1, Pallas kernels: 34.1 us -> 33.5 us  [body(): pl.pallas_call(functools.partial(kernel, dims), out_shape=pltpu.VMEM((row...]
where the time goes in v1:
time: 34.3 us; the launch traced here: 34.1 us
  Pallas kernels  33.5 us (98%)
  local copies, waits for them, and re-layouts  0.62 us (2%)
    pallas_call x1, Pallas kernels, body(): pl.pallas_call(functools.partial(kernel, dims), out_shape=pltpu.VMEM((row...  33.5 us

profile of v1, /device:TPU:0, one launch (start us, length us, event | category | flops | bytes accessed | tf_op | source)
XLA Modules:
  0.0 34.1 jit_solution(7614748712059889625)
XLA Ops:
  0.0 33.5 %shard_map.82 = bf16[32,512]{1,0:T(8,128)(2,1)S(1)} custom-call(bf16[32,2048]{1,0:T(8,128)(2,1)} %tokens_hbm.1, f32[1,2048]{1,0:T(1,128)} %bitcast.4, f32[1,2048]{1,0:T(1,128)} %bitcast.5, s32[4,32]{1,0:T(4,128)} %bitcast.6, f32[4,32]{1,0:T(4,128)} %bitcast.7, bf16[1,2048,1024]{2,1,0:T(8,128)(2,1)} %gate_hbm.1, bf16[1,2048,1024]{2,1,0:T(8,128)(2,1)} %up_hbm.1, ...), custom_call_target="tpu_custom_call" | custom-call | tf_op jit(solution)/shard_map/pallas_call | solution.py:392
  33.5 0.6 %copy.10 = bf16[32,512]{1,0:T(8,128)(2,1)} copy(bf16[32,512]{1,0:T(8,128)(2,1)S(1)} %shard_map.82) | data formatting | bytes 65536
